TPU v7x, 512 devices: a whole 4x4x16 slice. The times are simulated.
512 devices in a mesh: vp: 128 (over z, x, core), dp: 4 (over y).
Axes of the slice: x: 4, y: 4, z: 16, core: 2. Of those that a mesh axis runs over, the one named last changes fastest.
Arguments:
- stream: bfloat16 [1024, 2048], P(('dp', 'vp')), may hold values from -60 to 60
- hidden: bfloat16 [1024, 5632], P('dp', 'vp'), may hold values from -6 to 6
- w_down: bfloat16 [5632, 2048], P(None, 'vp'), may hold values from -0.078125 to 0.078125
- final_gain: float32 [2048], replicated, may hold values from 0.1 to 1.9
- vocab: bfloat16 [2048, 32768], P(None, 'vp'), may hold values from -2 to 200
- vocab_bias: float32 [32768], P('vp'), may hold values from -5 to 5
- targets: int32 [1024], P('dp'), may hold values from 0 to 32767
Outputs:
- losses: float32 [1024], P(('dp', 'vp'))
- grad_input: float32 [1024, 2048], P(('dp', 'vp'))
- grad_vocab: float32 [2048, 32768], P('dp', 'vp')
All inputs are finite; a program needn't handle non-finite values.
Results may differ from a plain program's by a relative error of at most 0.02.
Values may be sent and summed in bfloat16 or wider, within the bound.
No kernel may reach another device: no remote copies, remote signals or barrier semaphores. Data moves between devices by JAX's collectives and lax.ppermute only.
A program may use at most 64 MiB of HBM per device.

v0:
```python
import jax
import jax.numpy as jnp
from jax import lax
from jax.sharding import Mesh
from jax.sharding import PartitionSpec as P

VP = ("vp_0", "vp_1", "vp_2")
DP_VP = ("dp", "vp_0", "vp_1", "vp_2")
norm_eps = 1e-06
zloss_weight = 0.001


def joined_along(pieces, dim):
    pieces = jnp.moveaxis(pieces, 0, dim)
    lengths = pieces.shape
    return pieces.reshape(*lengths[:dim], lengths[dim] * lengths[dim + 1], *lengths[dim + 2 :])


def gather_in_order(array, axes, turns):
    pieces = array[None]
    for k in turns:
        pieces = lax.all_gather(pieces, axes[k], axis=0, tiled=True)
    held = [lax.axis_size(axes[k]) for k in reversed(turns)]
    pieces = pieces.reshape(*held, *array.shape)
    turned = sorted(range(len(turns)), key=lambda place: turns[len(turns) - 1 - place])
    return pieces.transpose(*turned, *range(len(turns), pieces.ndim)).reshape(-1, *array.shape)


def whole_of(array, axes, turns, dim):
    return joined_along(gather_in_order(array, axes, turns), dim)


def collected_together(array, axis):
    leaves = jax.tree.leaves(array)
    turns = sorted(range(len(leaves)), key=lambda k: -leaves[k].size)
    width = (1, *leaves[turns[0]].shape)[-1]
    lines = [
        jnp.pad(leaves[k].reshape(-1), (0, -leaves[k].size % width)).reshape(-1, width)
        for k in turns
    ]
    both, at, found = (lax.all_gather(jnp.concatenate(lines), axis), 0, {})
    for k, line in zip(turns, lines):
        section = both[:, at : at + len(line)].reshape(len(both), -1)
        found[k] = section[:, : leaves[k].size].reshape(-1, *leaves[k].shape)
        at += len(line)
    numbers = iter(range(len(leaves)))
    return jax.tree.map(lambda _: found[next(numbers)], array)


def merged_by_axis(array, axes, combine):
    for axis in axes:
        pieces = collected_together(array, axis)
        array = jax.tree.map(lambda part: part[0], pieces)
        for k in range(1, lax.axis_size(axis)):
            array = combine(array, jax.tree.map(lambda part: part[k], pieces))
    return array


def sent_together(arrays, axis, dim, along):
    ends, at = ([], 0)
    for a in arrays[:-1]:
        at += a.shape[along]
        ends.append(at)
    both = jnp.concatenate(arrays, axis=along)
    return tuple(jnp.split(lax.all_gather(both, axis, axis=dim, tiled=True), ends, axis=along))


def combine_stats(first, second):
    top = jnp.maximum(first[0], second[0])
    total = first[1] * jnp.exp(first[0] - top) + second[1] * jnp.exp(second[0] - top)
    return (top, total, first[2] + second[2])


def body(stream, hidden, w_down, final_gain, vocab, vocab_bias, targets):
    rows_dev = stream.shape[0]
    width = stream.shape[1]
    group = targets.shape[0]
    mine = lax.axis_index(VP)
    w_rows = lax.all_to_all(w_down, VP, split_axis=0, concat_axis=1, tiled=True)
    partial_value = jnp.dot(hidden, w_rows, preferred_element_type=jnp.float32)
    arrived = lax.all_to_all(partial_value[:, None, :], VP, split_axis=0, concat_axis=1, tiled=True)
    proj = jnp.sum(arrived, axis=1)
    normin = (stream.astype(jnp.float32) + proj).astype(jnp.bfloat16)
    values = normin.astype(jnp.float32)
    inv = lax.rsqrt(jnp.mean(values * values, axis=1, keepdims=True) + norm_eps)
    normed_own = (values * inv * final_gain).astype(jnp.bfloat16)
    normed = whole_of(normed_own, VP, (1, 0, 2), 0)
    ncols = vocab.shape[1]
    scores = jnp.dot(normed, vocab, preferred_element_type=jnp.float32) + vocab_bias
    local_top = jnp.max(scores, axis=1)
    local_total = jnp.sum(jnp.exp(scores - local_top[:, None]), axis=1)
    column_ids = lax.broadcasted_iota(jnp.int32, (group, ncols), 1) + mine * ncols
    hit = column_ids == targets[:, None]
    local_target = jnp.sum(jnp.where(hit, scores, 0.0), axis=1)
    top, total, target_score = merged_by_axis(
        (local_top, local_total, local_target), VP, combine_stats
    )
    lse = top + jnp.log(total)
    group_losses = lse - target_score + zloss_weight * lse * lse
    losses = lax.dynamic_slice_in_dim(group_losses, mine * rows_dev, rows_dev)
    probs = jnp.exp(scores - lse[:, None])
    dscore = (probs * (1.0 + 2.0 * zloss_weight * lse)[:, None] - jnp.where(hit, 1.0, 0.0)).astype(
        jnp.bfloat16
    )
    feat_group = width // lax.axis_size("dp")
    feat_start = lax.axis_index("dp") * feat_group
    pieces = sent_together((normed, dscore), "dp", 0, 1)
    rows_slice = lax.dynamic_slice_in_dim(pieces[0], feat_start, feat_group, 1)
    grad_vocab = lax.dot_general(
        rows_slice, pieces[1], (((0,), (0,)), ((), ())), preferred_element_type=jnp.float32
    )
    row_term = lax.dot_general(
        dscore, vocab, (((1,), (1,)), ((), ())), preferred_element_type=jnp.float32
    )
    row_parts = lax.all_to_all(
        row_term[:, None, :].astype(jnp.bfloat16), VP, split_axis=0, concat_axis=1, tiled=True
    ).astype(jnp.float32)
    dnormed = jnp.sum(row_parts, axis=1)
    scaled = dnormed * final_gain
    grad_input = inv * (
        scaled - values * inv * inv * jnp.mean(values * scaled, axis=1, keepdims=True)
    )
    return (losses, grad_input, grad_vocab)


def solution(mesh):
    torus = Mesh(mesh.devices.reshape(16, 4, 2, mesh.shape["dp"]), ("vp_0", "vp_1", "vp_2", "dp"))
    return jax.shard_map(
        body,
        mesh=torus,
        in_specs=(P(DP_VP, None), P("dp", VP), P(None, VP), P(), P(None, VP), P(VP), P("dp")),
        out_specs=(P(DP_VP), P(DP_VP, None), P("dp", VP)),
        check_vma=False,
    )
```

profile of v0, /device:TPU:33, one launch (start us, length us, event | category | flops | bytes accessed | tf_op | source)
XLA Modules:
  0.0 378.1 jit_solution(5065636591865383652)
XLA Ops:
  7.2 2.5 all_to_all.30
  10.1 0.8 reshape.1388
  10.9 38.9 %all_to_all.40 = bf16[128,2,352]{2,1,0:T(2,128)(2,1)S(1)} all-to-all(bf16[128,2,352]{2,1,0:T(2,128)(2,1)S(1)} %reshape.1388), channel_id=1, replica_groups=mesh['vp_0'=16,'vp_1'=4,'vp_2'=2,'dp'=4] {'vp_0','vp_1','vp_2'}, dimensions={0} | all-to-all | bytes 360448 | tf_op jit(solution)/shard_map/all_to_all | solution.py:79
  50.8 2.2 copy.15
  53.0 105.4 %all_to_all.41 = f32[256,1,2048]{2,1,0:T(1,128)S(1)} all-to-all(f32[256,1,2048]{2,1,0:T(1,128)S(1)} %copy.15), channel_id=1, replica_groups=mesh['vp_0'=16,'vp_1'=4,'vp_2'=2,'dp'=4] {'vp_0','vp_1','vp_2'}, dimensions={0} | all-to-all | bytes 4194304 | tf_op jit(solution)/shard_map/all_to_all | solution.py:81
  158.3 6.8 %reduce.6 = f32[256,2048]{1,0:T(8,128)} reduce(f32[256,1,2048]{2,1,0:T(1,128)S(1)} %all_to_all.41, f32[]{:T(128)} %constant.50), dimensions={1}, to_apply=%all_to_all.34.reduce_sub_computation | reduce | bytes 4194308 | tf_op jit(solution)/shard_map/all_to_all | solution.py:81
  165.2 2.5 all_to_all.35
  168.7 9.1 %all-gather.4 = bf16[4,2,2048]{2,1,0:T(2,128)(2,1)S(1)} all-gather(bf16[1,2,2048]{2,1,0:T(2,128)(2,1)S(1)} %fusion.15), channel_id=2, replica_groups=mesh['vp_0'=16,'vp_1'=4,'vp_2'=2,'dp'=4] {'vp_1'}, dimensions={0}, use_global_device_ids=true | all-gather | bytes 40960 | tf_op jit(solution)/shard_map/all_gather | solution.py:22
  177.7 25.1 %all_gather.31 = bf16[64,2,2048]{2,1,0:T(2,128)(2,1)} all-gather(bf16[4,2,2048]{2,1,0:T(2,128)(2,1)S(1)} %all-gather.4), channel_id=1, replica_groups=mesh['vp_0'=16,'vp_1'=4,'vp_2'=2,'dp'=4] {'vp_0'}, dimensions={0}, use_global_device_ids=true | all-gather | bytes 557056 | tf_op jit(solution)/shard_map/all_gather | solution.py:22
  202.9 24.3 %all-gather.11.cloned.1.call-done = bf16[128,2,2048]{2,1,0:T(2,128)(2,1)} async-done(((bf16[64,2,2048]{2,1,0:T(2,128)(2,1)}), bf16[128,2,2048]{2,1,0:T(2,128)(2,1)}) %all-gather.11.cloned.1.call-update) | async-done | bytes 1048592 | tf_op jit(solution)/shard_map/all_gather | solution.py:22
  227.3 2.4 copy.23
  230.9 22.2 %all-gather.5 = f32[16,3,256]{2,1,0:T(4,128)S(1)} all-gather(f32[1,3,256]{2,1,0:T(4,128)S(1)} %maximum_bitcast_fusion), channel_id=3, replica_groups=mesh['vp_0'=16,'vp_1'=4,'vp_2'=2,'dp'=4] {'vp_0'}, dimensions={0}, use_global_device_ids=true | all-gather | bytes 52224 | tf_op jit(solution)/shard_map/all_gather | solution.py:41
  253.2 9.4 %all-gather.6 = f32[4,3,256]{2,1,0:T(4,128)S(1)} all-gather(f32[1,3,256]{2,1,0:T(4,128)S(1)} %maximum_bitcast_fusion.1), channel_id=4, replica_groups=mesh['vp_0'=16,'vp_1'=4,'vp_2'=2,'dp'=4] {'vp_1'}, dimensions={0}, use_global_device_ids=true | all-gather | bytes 15360 | tf_op jit(solution)/shard_map/all_gather | solution.py:41
  262.7 11.5 %all-gather.7 = f32[2,3,256]{2,1,0:T(4,128)S(1)} all-gather(f32[1,3,256]{2,1,0:T(4,128)S(1)} %maximum_bitcast_fusion.2), channel_id=5, replica_groups=mesh['vp_0'=16,'vp_1'=4,'vp_2'=2,'dp'=4] {'vp_2'}, dimensions={0}, use_global_device_ids=true | all-gather | bytes 9216 | tf_op jit(solution)/shard_map/all_gather | solution.py:41
  274.5 1.1 pad_maximum_fusion
  276.6 1.4 reduce.9
  278.0 1.5 reshape.1390
  279.5 14.1 %all-to-all-start.2 = ((bf16[128,2,2048]{2,1,0:T(2,128)(2,1)}), bf16[128,2,2048]{2,1,0:T(2,128)(2,1)}, u32[]{:S(2)}, u32[]{:S(2)}) async-start(bf16[128,2,2048]{2,1,0:T(2,128)(2,1)} %reshape.1390), calls=%async_computation.2 | async-start | bytes 2097152 | tf_op jit(solution)/shard_map/all_to_all | solution.py:115
  294.2 54.6 %all-to-all-done.2 = bf16[128,2,2048]{2,1,0:T(2,128)(2,1)} async-done(((bf16[128,2,2048]{2,1,0:T(2,128)(2,1)}), bf16[128,2,2048]{2,1,0:T(2,128)(2,1)}, u32[]{:S(2)}, u32[]{:S(2)}) %all-to-all-start.2) | async-done | bytes 1048608 | tf_op jit(solution)/shard_map/all_to_all | solution.py:115
  348.8 6.5 %reshape.1391 = bf16[256,1,2048]{2,1,0:T(2,128)(2,1)S(1)} reshape(bf16[128,2,2048]{2,1,0:T(2,128)(2,1)} %all-to-all-done.2) | data formatting | bytes 2097152
  355.3 7.4 %convert_reduce_fusion = f32[256,2048]{1,0:T(8,128)} fusion(bf16[256,1,2048]{2,1,0:T(2,128)(2,1)S(1)} %reshape.1391), kind=kLoop, calls=%fused_computation.3 | loop fusion | flops 524288 | bytes 3145728 | tf_op jit(solution)/shard_map/convert_element_type | solution.py:117
  362.7 2.5 reshape.1359
  366.7 2.2 slice-done
  368.9 2.3 fusion.1
  (48 shorter events, 7.1 us)
Async XLA Ops:
  7.2 223.0 %copy-start = (bf16[2048,256]{1,0:T(8,128)(2,1)S(1)}, bf16[2048,256]{1,0:T(8,128)(2,1)}, u32[]{:S(2)}) copy-start(bf16[2048,256]{1,0:T(8,128)(2,1)} %param.11) | copy-start | bytes 3145732
  7.2 43.1 %copy-start.2 = (bf16[256,44]{0,1:T(8,128)(2,1)S(1)}, bf16[256,44]{0,1:T(8,128)(2,1)}, u32[]{:S(2)}) copy-start(bf16[256,44]{0,1:T(8,128)(2,1)} %param.8) | copy-start | bytes 67588
  7.2 220.1 %all-gather.11.cloned.1.call-start = ((), (), s32[]{:S(2)}) async-start(), calls=%async_computation.3 | async-start | bytes 1572864 | tf_op jit(solution)/shard_map/all_gather | solution.py:22
  167.7 0.8 copy-start.3
  167.7 0.9 copy-start.1
  202.9 163.8 %all-gather.13.cloned.1.call-start = ((), (), s32[]{:S(2)}) async-start(), calls=%async_computation.4 | async-start | bytes 5898240 | tf_op jit(solution)/shard_map/all_gather | solution.py:65
  227.3 2.9 copy-start.5
  229.7 1.1 copy-start.4
  279.5 69.3 %all-to-all-start.2 = ((bf16[128,2,2048]{2,1,0:T(2,128)(2,1)}), bf16[128,2,2048]{2,1,0:T(2,128)(2,1)}, u32[]{:S(2)}, u32[]{:S(2)}) async-start(bf16[128,2,2048]{2,1,0:T(2,128)(2,1)} %reshape.1390), calls=%async_computation.2 | async-start | bytes 2097152 | tf_op jit(solution)/shard_map/all_to_all | solution.py:115
  366.7 2.2 slice-start
Sparse Core Ops, SparseCore 0:
  203.0 24.2 all-gather.10
  275.7 58.3 all-gather.12
where the time goes:
time: 379 us; the launch traced here: 378 us
  blocking collectives  222 us (59%)
  waiting for transfers between devices  79 us (21%)
  local copies, waits for them, and re-layouts  25.6 us (7%)
  other arithmetic  19.6 us (5%)
  between operations  14.3 us (4%)
  starting transfers between devices  14.1 us (4%)
  matrix products  3.86 us (1%)
    all_to_all x1, blocking collectives, body(): lax.all_to_all(partial_value[:, None, :], VP, split_axis=0, concat_axis=1...  105 us
    all_to_all x1, waiting for transfers between devices, body(): lax.all_to_all(row_term[:, None, :].astype(jnp.bfloat16), VP, split_axis=...  54.6 us
    all_gather x3, blocking collectives, collected_together(): both, at, found = (lax.all_gather(jnp.concatenate(lines), axis), 0, {})  43.1 us
    all_to_all x1, blocking collectives, body(): w_rows = lax.all_to_all(w_down, VP, split_axis=0, concat_axis=1, tiled=True)  38.9 us
    all_gather x2, blocking collectives, gather_in_order(): pieces = lax.all_gather(pieces, axes[k], axis=0, tiled=True)  34.2 us
    all_gather x1, waiting for transfers between devices, gather_in_order(): pieces = lax.all_gather(pieces, axes[k], axis=0, tiled=True)  24.3 us
    all_to_all x1, starting transfers between devices, body(): lax.all_to_all(row_term[:, None, :].astype(jnp.bfloat16), VP, split_axis=...  14.1 us
    unnamed x16, local copies, waits for them, and re-layouts  9.37 us
  transfers between devices with their start and end apart: 3, of which 2 were waited for; matrix products, arithmetic and copies ran while one was open for 6% of the time, Pallas kernels for 0%

commit v1 on v0

--- a/solution.py
+++ b/solution.py
@@ -19,7 +19,10 @@
 def gather_in_order(array, axes, turns):
     pieces = array[None]
     for k in turns:
-        pieces = lax.all_gather(pieces, axes[k], axis=0, tiled=True)
+        count = lax.axis_size(axes[k])
+        blocks = jnp.stack([pieces for _ in range(count)])
+        blocks = lax.all_to_all(blocks, axes[k], split_axis=0, concat_axis=0)
+        pieces = jnp.concatenate(blocks, axis=0)
     held = [lax.axis_size(axes[k]) for k in reversed(turns)]
     pieces = pieces.reshape(*held, *array.shape)
     turned = sorted(range(len(turns)), key=lambda place: turns[len(turns) - 1 - place])

time: 379 us -> 362 us (0.955)
  blocking collectives: 222 us -> 202 us
    all_gather x2 -> x0, blocking collectives: 34.2 us -> none  [gather_in_order(): pieces = lax.all_gather(pieces, axes[k], axis=0, tiled=True)]
    all_to_all x0 -> x1, waiting for transfers between devices: none -> 24.6 us  [gather_in_order(): blocks = lax.all_to_all(blocks, axes[k], split_axis=0, concat_axis=0)]
    all_gather x1 -> x0, waiting for transfers between devices: 24.3 us -> none  [gather_in_order(): pieces = lax.all_gather(pieces, axes[k], axis=0, tiled=True)]
    all_to_all x0 -> x2, blocking collectives: none -> 16.1 us  [gather_in_order(): blocks = lax.all_to_all(blocks, axes[k], split_axis=0, concat_axis=0)]
    all_to_all x0 -> x1, starting transfers between devices: none -> 5.29 us  [gather_in_order(): blocks = lax.all_to_all(blocks, axes[k], split_axis=0, concat_axis=0)]
where the time goes in v1:
time: 362 us
  blocking collectives  202 us (56%)
  waiting for transfers between devices  79.2 us (22%)
  local copies, waits for them, and re-layouts  25.6 us (7%)
  other arithmetic  20.6 us (6%)
  starting transfers between devices  15.6 us (4%)
  between operations  14.3 us (4%)
  matrix products  3.86 us (1%)
    all_to_all x1, blocking collectives, body(): lax.all_to_all(partial_value[:, None, :], VP, split_axis=0, concat_axis=1...  105 us
    all_to_all x1, waiting for transfers between devices, body(): lax.all_to_all(row_term[:, None, :].astype(jnp.bfloat16), VP, split_axis=...  54.6 us
    all_gather x3, blocking collectives, collected_together(): both, at, found = (lax.all_gather(jnp.concatenate(lines), axis), 0, {})  42.1 us
    all_to_all x1, blocking collectives, body(): w_rows = lax.all_to_all(w_down, VP, split_axis=0, concat_axis=1, tiled=True)  38.9 us
    all_to_all x1, waiting for transfers between devices, gather_in_order(): blocks = lax.all_to_all(blocks, axes[k], split_axis=0, concat_axis=0)  24.6 us
    all_to_all x2, blocking collectives, gather_in_order(): blocks = lax.all_to_all(blocks, axes[k], split_axis=0, concat_axis=0)  16.1 us
    all_to_all x1, starting transfers between devices, body(): lax.all_to_all(row_term[:, None, :].astype(jnp.bfloat16), VP, split_axis=...  10.3 us
    unnamed x16, local copies, waits for them, and re-layouts  9.37 us
  transfers between devices with their start and end apart: 3, of which 2 were waited for; matrix products, arithmetic and copies ran while one was open for 6% of the time, Pallas kernels for 0%

profile of v1, /device:TPU:33, one launch (start us, length us, event | category | flops | bytes accessed | tf_op | source)
XLA Modules:
  0.0 361.6 jit_solution(3653035810607998083)
XLA Ops:
  7.2 2.5 all_to_all.39
  10.9 38.9 %all_to_all.55 = bf16[128,2,352]{2,1,0:T(2,128)(2,1)S(1)} all-to-all(bf16[128,2,352]{2,1,0:T(2,128)(2,1)S(1)} %reshape.1384), channel_id=1, replica_groups=mesh['vp_0'=16,'vp_1'=4,'vp_2'=2,'dp'=4] {'vp_0','vp_1','vp_2'}, dimensions={0} | all-to-all | bytes 360448 | tf_op jit(solution)/shard_map/all_to_all | solution.py:82
  50.8 2.2 copy.14
  52.9 105.4 %all_to_all.56 = f32[256,1,2048]{2,1,0:T(1,128)S(1)} all-to-all(f32[256,1,2048]{2,1,0:T(1,128)S(1)} %copy.14), channel_id=1, replica_groups=mesh['vp_0'=16,'vp_1'=4,'vp_2'=2,'dp'=4] {'vp_0','vp_1','vp_2'}, dimensions={0} | all-to-all | bytes 4194304 | tf_op jit(solution)/shard_map/all_to_all | solution.py:84
  158.3 6.8 %reduce.6 = f32[256,2048]{1,0:T(8,128)} reduce(f32[256,1,2048]{2,1,0:T(1,128)S(1)} %all_to_all.56, f32[]{:T(128)} %constant.50), dimensions={1}, to_apply=%all_to_all.43.reduce_sub_computation | reduce | bytes 4194308 | tf_op jit(solution)/shard_map/all_to_all | solution.py:84
  165.2 2.5 all_to_all.44
  168.7 6.7 %all_to_all.57 = bf16[4,1,2,2048]{3,2,1,0:T(2,128)(2,1)S(1)} all-to-all(bf16[4,1,2,2048]{3,2,1,0:T(2,128)(2,1)S(1)} %stack.9), channel_id=1, replica_groups=mesh['vp_0'=16,'vp_1'=4,'vp_2'=2,'dp'=4] {'vp_1'}, dimensions={0} | all-to-all | bytes 65536 | tf_op jit(solution)/shard_map/all_to_all | solution.py:24
  175.4 1.2 stack.10
  176.6 5.3 %all-to-all-start.3 = ((bf16[16,4,2,2048]{3,2,1,0:T(2,128)(2,1)}), bf16[16,4,2,2048]{3,2,1,0:T(2,128)(2,1)S(1)}, u32[]{:S(2)}, u32[]{:S(2)}) async-start(bf16[16,4,2,2048]{3,2,1,0:T(2,128)(2,1)} %stack.10), calls=%async_computation.3 | async-start | bytes 1048576 | tf_op jit(solution)/shard_map/all_to_all | solution.py:24
  181.9 24.6 %all-to-all-done.3 = bf16[16,4,2,2048]{3,2,1,0:T(2,128)(2,1)S(1)} async-done(((bf16[16,4,2,2048]{3,2,1,0:T(2,128)(2,1)}), bf16[16,4,2,2048]{3,2,1,0:T(2,128)(2,1)S(1)}, u32[]{:S(2)}, u32[]{:S(2)}) %all-to-all-start.3) | async-done | bytes 524320 | tf_op jit(solution)/shard_map/all_to_all | solution.py:24
  207.5 9.4 %all_to_all.58 = bf16[2,64,2,2048]{3,2,1,0:T(2,128)(2,1)S(1)} all-to-all(bf16[2,64,2,2048]{3,2,1,0:T(2,128)(2,1)S(1)} %pad_maximum_fusion.1), channel_id=1, replica_groups=mesh['vp_0'=16,'vp_1'=4,'vp_2'=2,'dp'=4] {'vp_2'}, dimensions={0} | all-to-all | bytes 2097152 | tf_op jit(solution)/shard_map/all_to_all | solution.py:24
  216.9 1.2 copy.22
  219.3 21.2 %all-gather.3 = f32[16,3,256]{2,1,0:T(4,128)S(1)} all-gather(f32[1,3,256]{2,1,0:T(4,128)S(1)} %maximum_bitcast_fusion), channel_id=2, replica_groups=mesh['vp_0'=16,'vp_1'=4,'vp_2'=2,'dp'=4] {'vp_0'}, dimensions={0}, use_global_device_ids=true | all-gather | bytes 52224 | tf_op jit(solution)/shard_map/all_gather | solution.py:44
  240.6 9.1 %all-gather.4 = f32[4,3,256]{2,1,0:T(4,128)S(1)} all-gather(f32[1,3,256]{2,1,0:T(4,128)S(1)} %maximum_bitcast_fusion.1), channel_id=3, replica_groups=mesh['vp_0'=16,'vp_1'=4,'vp_2'=2,'dp'=4] {'vp_1'}, dimensions={0}, use_global_device_ids=true | all-gather | bytes 15360 | tf_op jit(solution)/shard_map/all_gather | solution.py:44
  249.8 11.8 %all-gather.5 = f32[2,3,256]{2,1,0:T(4,128)S(1)} all-gather(f32[1,3,256]{2,1,0:T(4,128)S(1)} %maximum_bitcast_fusion.2), channel_id=4, replica_groups=mesh['vp_0'=16,'vp_1'=4,'vp_2'=2,'dp'=4] {'vp_2'}, dimensions={0}, use_global_device_ids=true | all-gather | bytes 9216 | tf_op jit(solution)/shard_map/all_gather | solution.py:44
  263.9 1.4 reduce.9
  265.3 1.5 reshape.1386
  266.9 10.3 %all-to-all-start.5 = ((bf16[128,2,2048]{2,1,0:T(2,128)(2,1)}), bf16[128,2,2048]{2,1,0:T(2,128)(2,1)}, u32[]{:S(2)}, u32[]{:S(2)}) async-start(bf16[128,2,2048]{2,1,0:T(2,128)(2,1)} %reshape.1386), calls=%async_computation.5 | async-start | bytes 2097152 | tf_op jit(solution)/shard_map/all_to_all | solution.py:118
  277.8 54.6 %all-to-all-done.5 = bf16[128,2,2048]{2,1,0:T(2,128)(2,1)} async-done(((bf16[128,2,2048]{2,1,0:T(2,128)(2,1)}), bf16[128,2,2048]{2,1,0:T(2,128)(2,1)}, u32[]{:S(2)}, u32[]{:S(2)}) %all-to-all-start.5) | async-done | bytes 1048608 | tf_op jit(solution)/shard_map/all_to_all | solution.py:118
  332.4 6.5 %reshape.1387 = bf16[256,1,2048]{2,1,0:T(2,128)(2,1)S(1)} reshape(bf16[128,2,2048]{2,1,0:T(2,128)(2,1)} %all-to-all-done.5) | data formatting | bytes 2097152
  338.9 7.4 %convert_reduce_fusion = f32[256,2048]{1,0:T(8,128)} fusion(bf16[256,1,2048]{2,1,0:T(2,128)(2,1)S(1)} %reshape.1387), kind=kLoop, calls=%fused_computation.3 | loop fusion | flops 524288 | bytes 3145728 | tf_op jit(solution)/shard_map/convert_element_type | solution.py:120
  346.2 2.5 reshape.1359
  350.3 2.2 slice-done
  352.5 2.3 fusion.1
  (50 shorter events, 9.9 us)
Async XLA Ops:
  7.2 211.4 %copy-start = (bf16[2048,256]{1,0:T(8,128)(2,1)S(1)}, bf16[2048,256]{1,0:T(8,128)(2,1)}, u32[]{:S(2)}) copy-start(bf16[2048,256]{1,0:T(8,128)(2,1)} %param.11) | copy-start | bytes 3145732
  7.2 43.1 %copy-start.2 = (bf16[256,44]{0,1:T(8,128)(2,1)S(1)}, bf16[256,44]{0,1:T(8,128)(2,1)}, u32[]{:S(2)}) copy-start(bf16[256,44]{0,1:T(8,128)(2,1)} %param.8) | copy-start | bytes 67588
  167.7 0.8 copy-start.3
  167.7 0.9 copy-start.1
  176.6 30.0 %all-to-all-start.3 = ((bf16[16,4,2,2048]{3,2,1,0:T(2,128)(2,1)}), bf16[16,4,2,2048]{3,2,1,0:T(2,128)(2,1)S(1)}, u32[]{:S(2)}, u32[]{:S(2)}) async-start(bf16[16,4,2,2048]{3,2,1,0:T(2,128)(2,1)} %stack.10), calls=%async_computation.3 | async-start | bytes 1048576 | tf_op jit(solution)/shard_map/all_to_all | solution.py:24
  181.9 168.4 %all-gather.8.cloned.1.call-start = ((), (), s32[]{:S(2)}) async-start(), calls=%async_computation.6 | async-start | bytes 5898240 | tf_op jit(solution)/shard_map/all_gather | solution.py:68
  216.9 1.6 copy-start.5
  218.1 1.1 copy-start.4
  266.9 65.5 %all-to-all-start.5 = ((bf16[128,2,2048]{2,1,0:T(2,128)(2,1)}), bf16[128,2,2048]{2,1,0:T(2,128)(2,1)}, u32[]{:S(2)}, u32[]{:S(2)}) async-start(bf16[128,2,2048]{2,1,0:T(2,128)(2,1)} %reshape.1386), calls=%async_computation.5 | async-start | bytes 2097152 | tf_op jit(solution)/shard_map/all_to_all | solution.py:118
  350.3 2.2 slice-start
Sparse Core Ops, SparseCore 0:
  263.0 54.7 all-gather.7
